TPU v7x, 32 devices: a whole 2x2x4 slice. The times are simulated.
32 devices in a mesh: grp: 2 (over x), ep: 16 (over z, y, core).
Axes of the slice: x: 2, y: 2, z: 4, core: 2. Of those that a mesh axis runs over, the one named last changes fastest.
Arguments:
- tokens: bfloat16 [128, 2048], P(('grp', 'ep')), parts along dimension 0, may hold values from -6 to 6
- lengths: int32 [128], P(('grp', 'ep')), parts along dimension 0, may hold values from 128 to 1024, as said below
- cache_key: bfloat16 [128, 1024, 256], P(('grp', 'ep')), parts along dimension 0, may hold values from -6 to 6
- cache_value: bfloat16 [128, 1024, 256], P(('grp', 'ep')), parts along dimension 0, may hold values from -6 to 6
- routes: int32 [128, 2], P(('grp', 'ep')), parts along dimension 0, may hold values from 0 to 3, all different within a row
- route_logits: float32 [128, 2], P(('grp', 'ep')), parts along dimension 0, may hold values from -6 to 6
- mix_gain: float32 [2048], replicated, may hold values from 0.1 to 1.9
- query_gain: float32 [64], replicated, may hold values from 0.1 to 1.9
- key_gain: float32 [64], replicated, may hold values from 0.1 to 1.9
- head_bias: float32 [16], replicated, may hold values from -9 to -3.5
- w_query: bfloat16 [2048, 1024], P('ep'), may hold values from -0.125 to 0.125
- w_key: bfloat16 [2048, 256], P('ep'), may hold values from -0.125 to 0.125
- w_value: bfloat16 [2048, 256], P('ep'), may hold values from -0.125 to 0.125
- w_out: bfloat16 [1024, 2048], P(None, 'ep'), may hold values from -0.1875 to 0.1875
- ffn_gain: float32 [2048], replicated, may hold values from 0.1 to 1.9
- w_gate: bfloat16 [2048, 28672], P(None, 'ep'), may hold values from -0.125 to 0.125
- w_up: bfloat16 [2048, 28672], P(None, 'ep'), may hold values from -0.125 to 0.125
- w_down: bfloat16 [28672, 2048], P('ep'), may hold values from -0.0625 to 0.0625
Outputs:
- output: bfloat16 [128, 2048], P(('grp', 'ep')), parts along dimension 0
- new_key: bfloat16 [128, 256], P(('grp', 'ep')), parts along dimension 0
- new_value: bfloat16 [128, 256], P(('grp', 'ep')), parts along dimension 0
There are 2 independent parts, one for each index of `grp`. A program takes and returns all parts, laid end to end along the dimension named above; an argument that names none is the same for every part. Nothing has to cross between parts.
Inputs may be any that keep to these rules, and one draw needn't show every extreme that they name: `lengths`: some sequence has all 1024 positions live.
All inputs are finite; a program needn't handle non-finite values.
Results may differ from a plain program's by a relative error of at most 0.0085.
Values may be sent and summed in bfloat16 or wider, within the bound.
No kernel may reach another device: no remote copies, remote signals or barrier semaphores. Data moves between devices by JAX's collectives and lax.ppermute only.
A program may use at most 128 MiB of HBM per device.

v0:
```python
import functools

import jax
import jax.numpy as jnp
from jax import lax
from jax.experimental import pallas as pl
from jax.experimental.pallas import tpu as pltpu
from jax.sharding import PartitionSpec as P


HEADS = 16
KV_HEADS = 4
HEAD_DIM = 64
FF = 7168
EPSILON = 1e-06

GROUP = HEADS // KV_HEADS
KEY_WIDTH = KV_HEADS * HEAD_DIM
QUERY_WIDTH = HEADS * HEAD_DIM
BLOCK = 256
FIRST = 2
SECOND = 0
F32 = jnp.float32
BF16 = jnp.bfloat16
VMEM = pltpu.VMEM
NT = (((1,), (1,)), ((), ()))


def vmem_spec():
    return pl.BlockSpec(memory_space=VMEM)


def stage_kernel(
    lengths_hbm,
    routes_hbm,
    logits_hbm,
    bias_hbm,
    qgain_hbm,
    kgain_hbm,
    mix_gain_hbm,
    ffn_gain_hbm,
    tokens_hbm,
    wq_hbm,
    wk_hbm,
    wv_hbm,
    w_out_hbm,
    key_hbm,
    my_gain_ref,
    scale_ref,
    column_ref,
    head_gain_ref,
    share_ref,
    ffn_gain_ref,
    w_in_ref,
    w_out_ref,
    key_ref,
    lengths_scr,
    routes_scr,
    logits_scr,
    bias_scr,
    head_gain_scr,
    mix_gain_scr,
    tokens_scr,
    sems,
):
    tokens = tokens_hbm.shape[0]
    small = [
        (lengths_hbm, lengths_scr),
        (routes_hbm, routes_scr),
        (logits_hbm, logits_scr),
        (bias_hbm, bias_scr),
        (qgain_hbm, head_gain_scr.at[0]),
        (kgain_hbm, head_gain_scr.at[1]),
        (mix_gain_hbm, mix_gain_scr),
        (tokens_hbm, tokens_scr),
    ]
    large = [(ffn_gain_hbm, ffn_gain_ref)]
    start = 0
    for source in (wq_hbm, wk_hbm, wv_hbm):
        large.append((source, w_in_ref.at[:, start : start + source.shape[1]]))
        start += source.shape[1]
    large += [
        (w_out_hbm, w_out_ref),
        (key_hbm, key_ref),
    ]
    copies = [
        pltpu.make_async_copy(source, target, sems.at[index])
        for index, (source, target) in enumerate(small + large)
    ]
    for copy in copies:
        copy.start()
    for copy in copies[: len(small)]:
        copy.wait()

    chip = lax.axis_index("ep") // 2
    my_gain_ref[...] = mix_gain_scr[pl.ds(2 * chip, 2), :]
    own = tokens_scr[...].astype(F32)
    token_scale = lax.rsqrt(jnp.mean(own * own, axis=-1, keepdims=True) + EPSILON)
    scale_ref[...] = jnp.broadcast_to(token_scale, scale_ref.shape)
    for index in range(2):
        head_gain_ref[index : index + 1, :] = jnp.concatenate(
            [head_gain_scr[index]] * KV_HEADS, axis=-1
        )

    columns = tokens * HEADS
    column = lax.broadcasted_iota(jnp.int32, column_ref[0:1, :].shape, 1)
    live = jnp.zeros(column.shape, jnp.int32)
    bias = jnp.zeros(column.shape, F32)
    for token in range(tokens):
        live = jnp.where(column % columns // HEADS == token, lengths_scr[token], live)
    for head in range(HEADS):
        bias = jnp.where(column % HEADS == head, bias_scr[head], bias)
    live = live - jnp.where(column >= columns, key_hbm.shape[1] // 2, 0)
    column_ref[0:1, :] = live.astype(F32)
    column_ref[1:2, :] = bias

    row = lax.broadcasted_iota(jnp.int32, share_ref.shape, 0)
    lane = lax.broadcasted_iota(jnp.int32, share_ref.shape, 1)
    first = jnp.zeros(share_ref.shape, jnp.int32)
    second = jnp.zeros(share_ref.shape, jnp.int32)
    gap = jnp.zeros(share_ref.shape, F32)
    for token in range(tokens):
        first = jnp.where(row == token, routes_scr[0, token], first)
        second = jnp.where(row == token, routes_scr[1, token], second)
        gap = jnp.where(row == token, logits_scr[0, token] - logits_scr[1, token], gap)
    share = jnp.where(first == lane, jax.nn.sigmoid(gap), 0.0)
    share_ref[...] = share + jnp.where(second == lane, jax.nn.sigmoid(-gap), 0.0)
    for copy in copies[len(small) :]:
        copy.wait()


def project_kernel(rows_ref, gain_ref, w_ref, wq_ref, wk_ref, wv_ref, after_ref, out_ref):
    chips, tokens, width = rows_ref.shape
    share = width // 2
    rows = rows_ref[...].astype(F32).reshape(chips * tokens, width)
    first = rows[:, :share] * gain_ref[0:1, :]
    second = rows[:, share:] * gain_ref[1:2, :]
    even = lax.axis_index("ep") % 2 == 0
    own = jnp.where(even, first, second).astype(BF16)
    other = jnp.where(even, second, first).astype(BF16)
    start = 0
    for other_ref in (wq_ref, wk_ref, wv_ref):
        size = other_ref.shape[1]
        span = slice(start, start + size)
        part = jnp.dot(own, w_ref[:, span], preferred_element_type=F32)
        part = part + jnp.dot(other, other_ref[...], preferred_element_type=F32)
        out_ref[:, :, span] = part.astype(BF16).reshape(chips, tokens, size)
        start += size


def weight_copies(places, sems, *sources):
    wg_hbm, wu_hbm, wd_hbm = sources
    size = wd_hbm.shape[0]
    chunk = chunk_of(size)
    copies = {}
    for step, (wg_ref, wu_ref, wd_ref, offset) in places.items():
        span = slice(step * chunk, (step + 1) * chunk)
        place = slice(offset, offset + chunk)
        row = len(copies)
        copies[step] = [
            pltpu.make_async_copy(wg_hbm.at[:, span], wg_ref.at[:, place], sems.at[row, 0]),
            pltpu.make_async_copy(wu_hbm.at[:, span], wu_ref.at[:, place], sems.at[row, 1]),
            pltpu.make_async_copy(wd_hbm.at[span, :], wd_ref.at[place, :], sems.at[row, 2]),
        ]
    return copies


def places_of(first, parts, chunk):
    count = parts[2].shape[0] // chunk
    return {first + index: (*parts, index * chunk) for index in range(count)}


def attend_kernel(
    parts_ref,
    scale_ref,
    column_ref,
    head_gain_ref,
    key_ref,
    value_hbm,
    wg_hbm,
    wu_hbm,
    wd_hbm,
    row_ref,
    new_key_ref,
    new_value_ref,
    wg_ref,
    wu_ref,
    wd_ref,
    heads_scr,
    value_ref,
    sem,
    sems,
):
    fetch = pltpu.make_async_copy(value_hbm, value_ref, sem)
    fetch.start()
    places = places_of(0, (wg_ref, wu_ref, wd_ref), chunk_of(wd_hbm.shape[0]))
    later = sum(weight_copies(places, sems, wg_hbm, wu_hbm, wd_hbm).values(), [])
    for copy in later:
        copy.start()
    shards, tokens, _ = parts_ref.shape
    cache_len = key_ref.shape[1]
    columns = tokens * HEADS

    total = parts_ref[0].astype(F32)
    for shard in range(1, shards):
        total = total + parts_ref[shard].astype(F32)
    total = total * scale_ref[:, 0:1]
    fresh_key = total[:, QUERY_WIDTH : QUERY_WIDTH + KEY_WIDTH]
    new_value_ref[...] = total[:, QUERY_WIDTH + KEY_WIDTH :].astype(BF16)

    lane = lax.broadcasted_iota(jnp.int32, (tokens, KEY_WIDTH), 1)
    squares = fresh_key * fresh_key
    key_scale = jnp.zeros_like(fresh_key)
    for head in range(KV_HEADS):
        mine = lane // HEAD_DIM == head
        mean = jnp.sum(jnp.where(mine, squares, 0.0), axis=-1, keepdims=True) / HEAD_DIM
        key_scale = jnp.where(mine, lax.rsqrt(mean + EPSILON), key_scale)
    new_key_ref[...] = (fresh_key * key_scale * head_gain_ref[1:2, :]).astype(BF16)

    for member in range(GROUP):
        pieces = []
        for group in range(KV_HEADS):
            head = group * GROUP + member
            pieces.append(total[:, head * HEAD_DIM : (head + 1) * HEAD_DIM])
        heads_scr[:, member, :] = jnp.concatenate(pieces, axis=-1)
    stacked = []
    for token in range(tokens):
        stacked += [heads_scr[token]] * KV_HEADS
    query = jnp.concatenate(stacked, axis=0)
    row = lax.broadcasted_iota(jnp.int32, query.shape, 0)
    col = lax.broadcasted_iota(jnp.int32, query.shape, 1)
    query = jnp.where(row % HEADS // GROUP == col // HEAD_DIM, query, 0.0)
    query_mean = jnp.sum(query * query, axis=-1, keepdims=True) / HEAD_DIM
    query = query * lax.rsqrt(query_mean + EPSILON) * head_gain_ref[0:1, :]
    query = query.astype(BF16).astype(F32)
    half = cache_len // 2
    blocks = half // BLOCK
    lower, upper = [], []
    for token in range(tokens):
        mine = jnp.where(row // HEADS == token, query, 0.0)
        lower.append(jnp.concatenate([mine, jnp.zeros_like(mine)], axis=0).astype(BF16))
        upper.append(jnp.concatenate([jnp.zeros_like(mine), mine], axis=0).astype(BF16))
    live = column_ref[0:1, :]
    bias = column_ref[1:2, :]
    after = (
        lax.broadcasted_iota(jnp.int32, (BLOCK, BLOCK), 1)
        >= lax.broadcasted_iota(jnp.int32, (BLOCK, BLOCK), 0)
    ).astype(F32).astype(BF16)
    scores = []
    for block in range(blocks):
        score = None
        for token in range(tokens):
            for start, side in ((0, lower), (half, upper)):
                span = slice(start + block * BLOCK, start + (block + 1) * BLOCK)
                part = lax.dot_general(
                    key_ref[token, span, :], side[token], NT, preferred_element_type=F32
                )
                score = part if score is None else score + part
        scores.append(score * HEAD_DIM ** (-0.5) + bias)
    sums = []
    for block in range(blocks):
        score = scores[block]
        spot = lax.broadcasted_iota(jnp.int32, score.shape, 0) + block * BLOCK
        remain = -(jnp.maximum(score, 0.0) + jnp.log1p(jnp.exp(-jnp.abs(score))))
        remain = jnp.where(spot.astype(F32) < live, remain, 0.0)
        high = remain.astype(BF16)
        low = (remain - high.astype(F32)).astype(BF16)
        sums.append(
            jnp.dot(after, high, preferred_element_type=F32)
            + jnp.dot(after, low, preferred_element_type=F32)
        )
    totals = [part[0:1, :] for part in sums]
    whole = functools.reduce(jnp.add, totals)
    lane = lax.broadcasted_iota(jnp.int32, whole.shape, 1)
    carry = jnp.where(lane < columns, jnp.concatenate([whole[:, columns:]] * 2, axis=-1), 0.0)
    weights = [None] * blocks
    for block in range(blocks - 1, -1, -1):
        score = scores[block]
        spot = lax.broadcasted_iota(jnp.int32, score.shape, 0) + block * BLOCK
        weight = jnp.exp(score + (sums[block] + carry))
        weight = jnp.where(spot.astype(F32) < live, weight, 0.0)
        weights[block] = weight.T.astype(BF16)
        carry = carry + totals[block]
    fetch.wait()
    attended = []
    for token in range(tokens):
        total_of = None
        for block in range(blocks):
            for start, line in ((0, 0), (half, columns)):
                span = slice(start + block * BLOCK, start + (block + 1) * BLOCK)
                first = line + token * HEADS
                part = jnp.dot(
                    weights[block][first : first + HEADS, :],
                    value_ref[token, span, :],
                    preferred_element_type=F32,
                )
                total_of = part if total_of is None else total_of + part
        attended.append(total_of)

    own_row = lax.broadcasted_iota(jnp.int32, (HEADS, KEY_WIDTH), 0)
    own_col = lax.broadcasted_iota(jnp.int32, (HEADS, KEY_WIDTH), 1)
    keep = own_row // GROUP == own_col // HEAD_DIM
    for token in range(tokens):
        kept = jnp.where(keep, attended[token], 0.0)
        folded = kept[0:GROUP]
        for group in range(1, KV_HEADS):
            folded = folded + kept[group * GROUP : (group + 1) * GROUP]
        heads_scr[token] = folded
    for member in range(GROUP):
        piece = heads_scr[:, member, :].astype(BF16)
        for shard in range(shards):
            row_ref[shard, :, member * KEY_WIDTH : (member + 1) * KEY_WIDTH] = piece

    for copy in later:
        copy.wait()


def mix_kernel(rows_ref, tokens_ref, own_ref, other_ref, mixed_ref):
    chips, tokens, width = tokens_ref.shape
    total, share = chips * tokens, width // 2
    rows = rows_ref[...].astype(F32).reshape(total, QUERY_WIDTH)
    rows = rows.astype(BF16)
    sides = []
    for w_ref in (own_ref, other_ref):
        side = jnp.zeros((total, share), F32)
        for member in range(GROUP):
            pieces = []
            for group in range(KV_HEADS):
                head = group * GROUP + member
                pieces.append(w_ref[head * HEAD_DIM : (head + 1) * HEAD_DIM, :])
            side = side + jnp.dot(
                rows[:, member * KEY_WIDTH : (member + 1) * KEY_WIDTH],
                jnp.concatenate(pieces, axis=0),
                preferred_element_type=F32,
            )
        sides.append(side)
    even = lax.axis_index("ep") % 2 == 0
    tokens_in = tokens_ref[...].astype(F32).reshape(total, width)
    first = (tokens_in[:, :share] + jnp.where(even, sides[0], sides[1])).astype(BF16)
    second = (tokens_in[:, share:] + jnp.where(even, sides[1], sides[0])).astype(BF16)
    for chip in range(chips):
        mixed_ref[chip, :, :share] = first
        mixed_ref[chip, :, share:] = second


def fetch_kernel(
    first, after_hbm, wg_hbm, wu_hbm, wd_hbm, wg_ref, wu_ref, wd_ref, sems
):
    places = places_of(first, (wg_ref, wu_ref, wd_ref), chunk_of(wd_hbm.shape[0]))
    copies = sum(weight_copies(places, sems, wg_hbm, wu_hbm, wd_hbm).values(), [])
    for copy in copies:
        copy.start()
    for copy in copies:
        copy.wait()


def chunk_of(size):
    return BLOCK if size % BLOCK == 0 else size


def expert_kernel(ready, own_mixed_ref, other_mixed_ref, gain_ref, *rest):
    heads, rest = rest[: 3 * ready], rest[3 * ready :]
    wg_hbm, wu_hbm, wd_hbm, own_ref, other_ref, mine_ref, *tail, sems = rest
    size = wd_hbm.shape[0]
    chunk = chunk_of(size)
    steps = size // chunk
    places = {}
    for index in range(0, 3 * ready, 3):
        places |= places_of(len(places), heads[index : index + 3], chunk)
    copies = {}
    if len(places) < steps:
        rest_of = places_of(len(places), tail, chunk)
        copies = weight_copies(rest_of, sems, wg_hbm, wu_hbm, wd_hbm)
        places |= rest_of
    for group in copies.values():
        for copy in group[:2]:
            copy.start()
    for group in copies.values():
        group[2].start()

    tokens = mine_ref.shape[0]
    half = own_ref.shape[0] * tokens
    sides = []
    for mixed_ref in (own_mixed_ref, other_mixed_ref):
        if len(mixed_ref.shape) == 3:
            pieces = [mixed_ref[chip].astype(F32) for chip in range(mixed_ref.shape[0])]
            sides.append(jnp.concatenate(pieces, axis=-1))
        else:
            sides.append(mixed_ref[...].astype(F32))
    me = lax.axis_index("ep")
    picked = lax.broadcasted_iota(jnp.int32, (tokens, half), 1) - me // 2 * tokens
    picked = picked == lax.broadcasted_iota(jnp.int32, (tokens, half), 0)
    mine_ref[...] = jnp.dot(
        picked.astype(F32).astype(BF16), sides[0].astype(BF16), preferred_element_type=F32
    )
    mixed = jnp.concatenate(sides, axis=0)
    scale = lax.rsqrt(jnp.mean(mixed * mixed, axis=-1, keepdims=True) + EPSILON)
    expert_in = (mixed * scale * gain_ref[...]).astype(BF16)
    result = None
    held = None
    waiting = []

    def project_down(result):
        for index, (hidden, wd_ref, place) in waiting:
            for copy in copies.get(index, [])[2:]:
                copy.wait()
            part = jnp.dot(hidden, wd_ref[place, :], preferred_element_type=F32)
            result = part if result is None else result + part
        waiting.clear()
        return result

    for step in range(steps + 1):
        fresh = None
        if step < steps:
            wg_ref, wu_ref, wd_ref, offset = places[step]
            place = slice(offset, offset + chunk)
            for copy in copies.get(step, [])[:2]:
                copy.wait()
            value = jnp.dot(expert_in, wg_ref[:, place], preferred_element_type=F32)
            up = jnp.dot(expert_in, wu_ref[:, place], preferred_element_type=F32)
            fresh = value, up, wd_ref, place
        if held is not None:
            value, up, wd_ref, place = held
            hidden = (value / (1.0 + jnp.exp(-value)) * up).astype(BF16)
            waiting.append((step - 1, (hidden, wd_ref, place)))
            if step - 1 not in copies:
                result = project_down(result)
        held = fresh
    result = project_down(result)
    own_ref[...] = result[:half].reshape(own_ref.shape)
    other_ref[...] = result[half:].astype(BF16).reshape(other_ref.shape)


def combine_kernel(own_ref, other_ref, out_ref):
    out_ref[...] = (own_ref[...] + other_ref[...].astype(F32)).astype(BF16)


def finish_kernel(
    size,
    parts_ref,
    gate_ref,
    mixed_ref,
    key_ref,
    value_ref,
    out_ref,
    new_key_ref,
    new_value_ref,
):
    new_key_ref[...] = key_ref[...]
    new_value_ref[...] = value_ref[...]
    total = mixed_ref[...]
    for chip in range(parts_ref.shape[0]):
        expert = 2 * chip // (FF // size)
        total = total + parts_ref[chip].astype(F32) * gate_ref[:, expert : expert + 1]
    out_ref[...] = total.astype(BF16)


def call(kernel, outs, specs, scratch=(), limit=20):
    return pl.pallas_call(
        kernel,
        out_shape=outs,
        in_specs=specs,
        out_specs=jax.tree.map(lambda _: vmem_spec(), outs),
        scratch_shapes=list(scratch),
        compiler_params=pltpu.CompilerParams(vmem_limit_bytes=limit << 20),
    )


def hbm_spec():
    return pl.BlockSpec(memory_space=pltpu.HBM)


def in_hbm(array):
    return pltpu.with_memory_space_constraint(array, pltpu.HBM)


def local(
    tokens,
    lengths,
    cache_key,
    cache_value,
    routes,
    route_logits,
    mix_gain,
    query_gain,
    key_gain,
    head_bias,
    w_query,
    w_key,
    w_value,
    w_out,
    ffn_gain,
    w_gate,
    w_up,
    w_down,
):
    shards = lax.axis_size("ep")
    chips = shards // 2
    token_rows, width = tokens.shape
    share = width // shards
    half_rows = chips * token_rows
    project_width = QUERY_WIDTH + 2 * KEY_WIDTH
    kept = pltpu.VMEM
    groups = [[2 * chip + core for chip in range(chips)] for core in range(2)]
    exchange = functools.partial(
        lax.all_to_all, axis_name="ep", split_axis=0, concat_axis=0, axis_index_groups=groups
    )
    mate = functools.partial(
        lax.ppermute, axis_name="ep", perm=[(index, index ^ 1) for index in range(shards)]
    )

    sliced = exchange(tokens.reshape(token_rows, chips, 2 * share).transpose(1, 0, 2))
    other_in = [mate(w_query), mate(w_key), mate(w_value)]
    other_out = mate(w_out)
    staged = [
        lengths,
        routes.T,
        route_logits.T,
        head_bias,
        query_gain[None, :],
        key_gain[None, :],
        mix_gain.reshape(shards, share),
        ffn_gain[None, :],
        tokens,
        w_query,
        w_key,
        w_value,
        w_out,
        cache_key,
    ]
    my_gain, scale, column, head_gain, gates, ffn_row, w_in, w_mix, key = call(
        stage_kernel,
        (
            kept((2, share), F32),
            kept((token_rows, 128), F32),
            kept((2, 2 * token_rows * HEADS), F32),
            kept((2, KEY_WIDTH), F32),
            kept((token_rows, 128), F32),
            kept((1, width), F32),
            kept((share, project_width), BF16),
            kept(w_out.shape, BF16),
            kept(cache_key.shape, BF16),
        ),
        [hbm_spec()] * len(staged),
        [
            pltpu.SMEM(lengths.shape, jnp.int32),
            pltpu.SMEM((2, token_rows), jnp.int32),
            pltpu.SMEM((2, token_rows), F32),
            pltpu.SMEM(head_bias.shape, F32),
            pltpu.VMEM((2, 1, HEAD_DIM), F32),
            pltpu.VMEM((shards, share), F32),
            pltpu.VMEM(tokens.shape, BF16),
            pltpu.SemaphoreType.DMA((len(staged),)),
        ],
        limit=4,
    )(*[in_hbm(array) for array in staged])
    parts = call(
        project_kernel,
        kept((chips, token_rows, project_width), BF16),
        [vmem_spec()] * 6 + [pl.BlockSpec(memory_space=pl.ANY)],
        limit=8,
    )(sliced, my_gain, w_in, *other_in, other_out)
    parts = exchange(parts)

    size = w_gate.shape[1]
    chunk = chunk_of(size)
    steps = size // chunk
    first = min(FIRST, steps)
    second = min(SECOND, steps - first)
    experts = [in_hbm(w_gate), in_hbm(w_up), in_hbm(w_down)]

    def triple(count, make):
        wide = count * chunk
        return tuple(make(shape, BF16) for shape in ((width, wide), (width, wide), (wide, width)))

    rows, new_key, new_value, *heads = call(
        attend_kernel,
        (
            kept((chips, token_rows, QUERY_WIDTH), BF16),
            kept((token_rows, KEY_WIDTH), BF16),
            kept((token_rows, KEY_WIDTH), BF16),
        )
        + triple(first, kept),
        [vmem_spec()] * 5 + [hbm_spec()] * 4,
        [
            pltpu.VMEM((token_rows, GROUP, KEY_WIDTH), F32),
            pltpu.VMEM(cache_value.shape, BF16),
            pltpu.SemaphoreType.DMA,
            pltpu.SemaphoreType.DMA((first, 3)),
        ],
    )(parts, scale, column, head_gain, key, in_hbm(cache_value), *experts)
    rows = exchange(rows)

    mixed = call(
        mix_kernel,
        kept((chips, half_rows, 2 * share), BF16),
        [vmem_spec()] * 4,
        limit=8,
    )(rows, sliced, w_mix, other_out)
    mixed = exchange(mixed)
    other_mixed = mate(mixed)
    if second:
        heads += call(
            functools.partial(fetch_kernel, first),
            triple(second, kept),
            [pl.BlockSpec(memory_space=pl.ANY)] + [hbm_spec()] * 3,
            [pltpu.SemaphoreType.DMA((second, 3))],
            limit=4,
        )(mixed, *experts)

    if 2 * share % 128:
        both = [side.transpose(1, 0, 2).reshape(half_rows, width) for side in (mixed, other_mixed)]
    else:
        both = [mixed, other_mixed]
    left = max(steps - first - second, 1)
    own, other, mine = call(
        functools.partial(expert_kernel, len(heads) // 3),
        (
            kept((chips, token_rows, width), F32),
            kept((chips, token_rows, width), BF16),
            kept((token_rows, width), F32),
        ),
        [vmem_spec()] * (3 + len(heads)) + [hbm_spec()] * 3,
        [*triple(left, pltpu.VMEM), pltpu.SemaphoreType.DMA((left, 3))],
        limit=28,
    )(*both, ffn_row, *heads, *experts)
    other = mate(other)
    sums = call(
        combine_kernel,
        kept((chips, token_rows, width), BF16),
        [vmem_spec()] * 2,
        limit=8,
    )(own, other)
    sums = exchange(sums)
    key_row = jax.ShapeDtypeStruct((token_rows, KEY_WIDTH), BF16)
    return call(
        functools.partial(finish_kernel, size),
        (jax.ShapeDtypeStruct((token_rows, width), BF16), key_row, key_row),
        [vmem_spec()] * 5,
        limit=8,
    )(sums, gates, mine, new_key, new_value)


def solution(mesh):
    return jax.shard_map(
        local,
        mesh=mesh,
        in_specs=(
            P(("grp", "ep"), None),
            P(("grp", "ep")),
            P(("grp", "ep"), None, None),
            P(("grp", "ep"), None, None),
            P(("grp", "ep"), None),
            P(("grp", "ep"), None),
            P(),
            P(),
            P(),
            P(),
            P("ep", None),
            P("ep", None),
            P("ep", None),
            P(None, "ep"),
            P(),
            P(None, "ep"),
            P(None, "ep"),
            P("ep", None),
        ),
        out_specs=(P(("grp", "ep"), None), P(("grp", "ep"), None), P(("grp", "ep"), None)),
        check_vma=False,
    )
```

profile of v0, /device:TPU:0, one launch (start us, length us, event | category | flops | bytes accessed | tf_op | source)
XLA Modules:
  0.0 68.2 jit_solution(2570729118803646043)
XLA Ops:
  0.6 0.6 collective-permute-start
  1.2 0.1 collective-permute-start.3
  1.3 0.4 collective-permute-start.1
  1.7 0.1 collective-permute-start.2
  1.8 7.2 %all-to-all-start = ((bf16[8,4,256]{2,1,0:T(4,128)(2,1)}), bf16[8,4,256]{2,1,0:T(4,128)(2,1)S(1)}, u32[]{:S(2)}, u32[]{:S(2)}) async-start(bf16[8,4,256]{2,1,0:T(4,128)(2,1)} %bitcast.9), calls=%async_computation | async-start | bytes 32768 | tf_op jit(solution)/shard_map/all_to_all | solution.py:512
  9.0 2.0 %shard_map.193 = (f32[2,128]{1,0:T(2,128)S(1)}, f32[4,128]{1,0:T(4,128)S(1)}, f32[2,128]{1,0:T(2,128)S(1)}, f32[2,256]{1,0:T(2,128)S(1)}, f32[4,128]{1,0:T(4,128...) custom-call(s32[4]{0:T(128)} %lengths_hbm.1, ...), custom_call_target="tpu_custom_call" | custom-call | tf_op jit(solution)/shard_map/pallas_call | solution.py:531
  11.1 4.5 %all-to-all-done.rows_ref.tokens_ref = bf16[8,4,256]{2,1,0:T(4,128)(2,1)S(1)} async-done(((bf16[8,4,256]{2,1,0:T(4,128)(2,1)}), bf16[8,4,256]{2,1,0:T(4,128)(2,1)S(1)}, u32[]{:S(2)}, u32[]{:S(2)}) %all-to-all-start) | async-done | bytes 16416 | tf_op jit(solution)/shard_map/all_to_all | solution.py:512
  15.6 0.0 collective-permute-done.1.wk_ref
  15.6 0.0 collective-permute-done.2.wv_ref
  15.6 0.0 collective-permute-done.wq_ref
  15.6 0.0 collective-permute-done.3.after_ref.other_ref
  15.6 0.2 shard_map.194
  15.9 9.5 %all_to_all.25.parts_ref = bf16[8,4,1536]{2,1,0:T(4,128)(2,1)S(1)} all-to-all(bf16[8,4,1536]{2,1,0:T(4,128)(2,1)S(1)} %shard_map.194), channel_id=1, replica_groups={{0,2,4,6,8,10,12,14},{1,3,5,7,9,11,13,15},{16,18,20,22,24,26,28,30},{17..., dimensions={0} | all-to-all | bytes 196608 | tf_op jit(solution)/shard_map/all_to_all | solution.py:563
  25.4 3.7 %shard_map.195 = (bf16[8,4,1024]{2,1,0:T(4,128)(2,1)S(1)}, bf16[4,256]{1,0:T(4,128)(2,1)S(1)}, bf16[4,256]{1,0:T(4,128)(2,1)S(1)}, bf16[2048,512]{1,0:T(8,128)(2...) custom-call(bf16[8,4,1536]{2,1,0:T(4,128)(2,1)S(1)} %all_to_all.25.parts_ref, ...), custom_call_target="tpu_custom_call" | custom-call | tf_op jit(solution)/shard_map/pallas_call | solution.py:576
  29.1 9.3 %all_to_all.26.rows_ref = bf16[8,4,1024]{2,1,0:T(4,128)(2,1)S(1)} all-to-all(bf16[8,4,1024]{2,1,0:T(4,128)(2,1)S(1)} %get-tuple-element.27), channel_id=1, replica_groups={{0,2,4,6,8,10,12,14},{1,3,5,7,9,11,13,15},{16,18,20,22,24,26,28,30},{17..., dimensions={0} | all-to-all | bytes 131072 | tf_op jit(solution)/shard_map/all_to_all | solution.py:592
  38.4 0.2 shard_map.196
  38.6 9.7 %all_to_all.27.own_mixed_ref = bf16[8,32,256]{2,1,0:T(8,128)(2,1)S(1)} all-to-all(bf16[8,32,256]{2,1,0:T(8,128)(2,1)S(1)} %shard_map.196), channel_id=1, replica_groups={{0,2,4,6,8,10,12,14},{1,3,5,7,9,11,13,15},{16,18,20,22,24,26,28,30},{17..., dimensions={0} | all-to-all | bytes 262144 | tf_op jit(solution)/shard_map/all_to_all | solution.py:600
  48.4 0.0 collective-permute-start.4
  48.4 1.3 %collective-permute-done.4.other_mixed_ref = bf16[8,32,256]{2,1,0:T(8,128)(2,1)S(1)} collective-permute-done((bf16[8,32,256]{2,1,0:T(8,128)(2,1)S(1)}, bf16[8,32,256]{2,1,0:T(8,128)(2,1)S(1)}, u32[]{:S(2)}, u32[]{:S(2)}) %collective-permute-start.4) | collective-permute-done | bytes 131104 | tf_op jit(solution)/shard_map/ppermute | solution.py:601
  49.7 6.3 %shard_map.197 = (f32[8,4,2048]{2,1,0:T(4,128)S(1)}, bf16[8,4,2048]{2,1,0:T(4,128)(2,1)S(1)}, f32[4,2048]{1,0:T(4,128)S(1)}) custom-call(bf16[8,32,256]{2,1,0:T(8,128)(2,1)S(1)} %all_to_all.27.own_mixed_ref, bf16[8,32,256]{2,1,0:T(8,128)(2,1)S(1)} %collective-permute-done.4.other_mixed_ref, f32[1,2048]{1,0:T(1,128)S(1)} %get-tuple-element.29.gain_ref, ...), custom_call_target="tpu_custom_call" | custom-call | tf_op jit(solution)/shard_map/pallas_call | solution.py:616
  56.0 0.2 collective-permute-start.5
  56.3 1.2 %collective-permute-done.5.other_ref = bf16[8,4,2048]{2,1,0:T(4,128)(2,1)S(1)} collective-permute-done((bf16[8,4,2048]{2,1,0:T(4,128)(2,1)S(1)}, bf16[8,4,2048]{2,1,0:T(4,128)(2,1)S(1)}, u32[]{:S(2)}, u32[]{:S(2)}) %collective-permute-start.5) | collective-permute-done | bytes 131104 | tf_op jit(solution)/shard_map/ppermute | solution.py:627
  57.5 0.1 shard_map.198
  57.5 10.0 %all_to_all.28.parts_ref = bf16[8,4,2048]{2,1,0:T(4,128)(2,1)S(1)} all-to-all(bf16[8,4,2048]{2,1,0:T(4,128)(2,1)S(1)} %shard_map.198), channel_id=1, replica_groups={{0,2,4,6,8,10,12,14},{1,3,5,7,9,11,13,15},{16,18,20,22,24,26,28,30},{17..., dimensions={0} | all-to-all | bytes 262144 | tf_op jit(solution)/shard_map/all_to_all | solution.py:634
  67.5 0.7 %shard_map.199 = (bf16[4,2048]{1,0:T(4,128)(2,1)}, bf16[4,256]{1,0:T(4,128)(2,1)}, bf16[4,256]{1,0:T(4,128)(2,1)}) custom-call(bf16[8,4,2048]{2,1,0:T(4,128)(2,1)S(1)} %all_to_all.28.parts_ref, f32[4,128]{1,0:T(4,128)S(1)} %get-tuple-element.35.gate_ref, f32[4,2048]{1,0:T(4,128)S(1)} %get-tuple-element.36.mixed_ref, ...), custom_call_target="tpu_custom_call" | custom-call | tf_op jit(solution)/shard_map/pallas_call | solution.py:636
Async XLA Ops:
  0.6 15.0 %collective-permute-start = (bf16[128,1024]{1,0:T(8,128)(2,1)}, bf16[128,1024]{1,0:T(8,128)(2,1)S(1)}, u32[]{:S(2)}, u32[]{:S(2)}) collective-permute-start(bf16[128,1024]{1,0:T(8,128)(2,1)} %wq_hbm.1), channel_id=1, source_target_pairs={{0,1},{1,0},{2,3},{3,2},{4,5},{5,4},{6,7},{7,6},{8,9},{9,8},{10,11... | collective-permute-start | bytes 786440 | tf_op jit(solution)/shard_map/ppermute | solution.py:513
  1.2 14.4 %collective-permute-start.3 = (bf16[1024,128]{1,0:T(8,128)(2,1)}, bf16[1024,128]{1,0:T(8,128)(2,1)S(1)}, u32[]{:S(2)}, u32[]{:S(2)}) collective-permute-start(bf16[1024,128]{1,0:T(8,128)(2,1)} %w_out_hbm.1), channel_id=1, source_target_pairs={{0,1},{1,0},{2,3},{3,2},{4,5},{5,4},{6,7},{7,6},{8,9},{9,8},{10,11... | collective-permute-start | bytes 786440 | tf_op jit(solution)/shard_map/ppermute | solution.py:514
  1.3 14.3 %collective-permute-start.1 = (bf16[128,256]{1,0:T(8,128)(2,1)}, bf16[128,256]{1,0:T(8,128)(2,1)S(1)}, u32[]{:S(2)}, u32[]{:S(2)}) collective-permute-start(bf16[128,256]{1,0:T(8,128)(2,1)} %wk_hbm.1), channel_id=1, source_target_pairs={{0,1},{1,0},{2,3},{3,2},{4,5},{5,4},{6,7},{7,6},{8,9},{9,8},{10,11... | collective-permute-start | bytes 196616 | tf_op jit(solution)/shard_map/ppermute | solution.py:513
  1.7 13.9 %collective-permute-start.2 = (bf16[128,256]{1,0:T(8,128)(2,1)}, bf16[128,256]{1,0:T(8,128)(2,1)S(1)}, u32[]{:S(2)}, u32[]{:S(2)}) collective-permute-start(bf16[128,256]{1,0:T(8,128)(2,1)} %wv_hbm.1), channel_id=1, source_target_pairs={{0,1},{1,0},{2,3},{3,2},{4,5},{5,4},{6,7},{7,6},{8,9},{9,8},{10,11... | collective-permute-start | bytes 196616 | tf_op jit(solution)/shard_map/ppermute | solution.py:513
  1.8 13.8 %all-to-all-start = ((bf16[8,4,256]{2,1,0:T(4,128)(2,1)}), bf16[8,4,256]{2,1,0:T(4,128)(2,1)S(1)}, u32[]{:S(2)}, u32[]{:S(2)}) async-start(bf16[8,4,256]{2,1,0:T(4,128)(2,1)} %bitcast.9), calls=%async_computation | async-start | bytes 32768 | tf_op jit(solution)/shard_map/all_to_all | solution.py:512
  48.4 1.3 %collective-permute-start.4 = (bf16[8,32,256]{2,1,0:T(8,128)(2,1)S(1)}, bf16[8,32,256]{2,1,0:T(8,128)(2,1)S(1)}, u32[]{:S(2)}, u32[]{:S(2)}) collective-permute-start(bf16[8,32,256]{2,1,0:T(8,128)(2,1)S(1)} %all_to_all.27.own_mixed_ref), channel_id=1, source_target_pairs={{0,1},{1,0},{2,3},{3,2},{4,5},{5,4},{6,7},{7,6},{8,9},{9,8},{10,11... | collective-permute-start | bytes 393224 | tf_op jit(solution)/shard_map/ppermute | solution.py:601
  56.0 1.4 %collective-permute-start.5 = (bf16[8,4,2048]{2,1,0:T(4,128)(2,1)S(1)}, bf16[8,4,2048]{2,1,0:T(4,128)(2,1)S(1)}, u32[]{:S(2)}, u32[]{:S(2)}) collective-permute-start(bf16[8,4,2048]{2,1,0:T(4,128)(2,1)S(1)} %get-tuple-element.34), channel_id=1, source_target_pairs={{0,1},{1,0},{2,3},{3,2},{4,5},{5,4},{6,7},{7,6},{8,9},{9,8},{10,11... | collective-permute-start | bytes 393224 | tf_op jit(solution)/shard_map/ppermute | solution.py:627
where the time goes:
time: 68.6 us; the launch traced here: 68.2 us
  blocking collectives  38.5 us (56%)
  Pallas kernels  13.3 us (19%)
  starting transfers between devices  8.61 us (13%)
  waiting for transfers between devices  7.1 us (10%)
  between operations  0.7 us (1%)
    all_to_all x1, blocking collectives, local(): sums = exchange(sums)  9.97 us
    all_to_all x1, blocking collectives, local(): mixed = exchange(mixed)  9.74 us
    all_to_all x1, blocking collectives, local(): parts = exchange(parts)  9.51 us
    all_to_all x1, blocking collectives, local(): rows = exchange(rows)  9.29 us
    all_to_all x1, starting transfers between devices, local(): exchange(tokens.reshape(token_rows, chips, 2 * share).transpose(1, 0, 2))  7.25 us
    pallas_call x1, Pallas kernels, local(): call(functools.partial(expert_kernel, len(heads) // 3), (kept((chips, tok...  6.32 us
    all_to_all x1, waiting for transfers between devices, local(): exchange(tokens.reshape(token_rows, chips, 2 * share).transpose(1, 0, 2))  4.55 us
    pallas_call x1, Pallas kernels, local(): call(attend_kernel, (kept((chips, token_rows, QUERY_WIDTH), BF16), kept((...  3.74 us
  transfers between devices with their start and end apart: 7, of which 3 were waited for; matrix products, arithmetic and copies ran while one was open for 0% of the time, Pallas kernels for 3%

commit v1 on v0

--- a/solution.py
+++ b/solution.py
@@ -19,7 +19,6 @@
 QUERY_WIDTH = HEADS * HEAD_DIM
 BLOCK = 256
 FIRST = 2
-SECOND = 0
 F32 = jnp.float32
 BF16 = jnp.bfloat16
 VMEM = pltpu.VMEM
@@ -343,22 +342,18 @@
         mixed_ref[chip, :, share:] = second
 
 
-def fetch_kernel(
-    first, after_hbm, wg_hbm, wu_hbm, wd_hbm, wg_ref, wu_ref, wd_ref, sems
-):
-    places = places_of(first, (wg_ref, wu_ref, wd_ref), chunk_of(wd_hbm.shape[0]))
-    copies = sum(weight_copies(places, sems, wg_hbm, wu_hbm, wd_hbm).values(), [])
-    for copy in copies:
-        copy.start()
-    for copy in copies:
-        copy.wait()
+def fetch_kernel(start, after_hbm, source_hbm, target_ref, sem):
+    span = slice(start, start + target_ref.shape[0])
+    copy = pltpu.make_async_copy(source_hbm.at[span, :], target_ref, sem)
+    copy.start()
+    copy.wait()
 
 
 def chunk_of(size):
     return BLOCK if size % BLOCK == 0 else size
 
 
-def expert_kernel(ready, own_mixed_ref, other_mixed_ref, gain_ref, *rest):
+def expert_kernel(ready, own_mixed_ref, other_mixed_ref, gain_ref, down_ref, *rest):
     heads, rest = rest[: 3 * ready], rest[3 * ready :]
     wg_hbm, wu_hbm, wd_hbm, own_ref, other_ref, mine_ref, *tail, sems = rest
     size = wd_hbm.shape[0]
@@ -372,11 +367,14 @@
         rest_of = places_of(len(places), tail, chunk)
         copies = weight_copies(rest_of, sems, wg_hbm, wu_hbm, wd_hbm)
         places |= rest_of
+        fetched = min(rest_of)
+        copies[fetched].pop()
     for group in copies.values():
         for copy in group[:2]:
             copy.start()
     for group in copies.values():
-        group[2].start()
+        for copy in group[2:]:
+            copy.start()
 
     tokens = mine_ref.shape[0]
     half = own_ref.shape[0] * tokens
@@ -418,7 +416,10 @@
                 copy.wait()
             value = jnp.dot(expert_in, wg_ref[:, place], preferred_element_type=F32)
             up = jnp.dot(expert_in, wu_ref[:, place], preferred_element_type=F32)
-            fresh = value, up, wd_ref, place
+            if len(copies.get(step, [0, 0, 0])) < 3:
+                fresh = value, up, down_ref, slice(0, chunk)
+            else:
+                fresh = value, up, wd_ref, place
         if held is not None:
             value, up, wd_ref, place = held
             hidden = (value / (1.0 + jnp.exp(-value)) * up).astype(BF16)
@@ -566,7 +567,6 @@
     chunk = chunk_of(size)
     steps = size // chunk
     first = min(FIRST, steps)
-    second = min(SECOND, steps - first)
     experts = [in_hbm(w_gate), in_hbm(w_up), in_hbm(w_down)]
 
     def triple(count, make):
@@ -599,20 +599,19 @@
     )(rows, sliced, w_mix, other_out)
     mixed = exchange(mixed)
     other_mixed = mate(mixed)
-    if second:
-        heads += call(
-            functools.partial(fetch_kernel, first),
-            triple(second, kept),
-            [pl.BlockSpec(memory_space=pl.ANY)] + [hbm_spec()] * 3,
-            [pltpu.SemaphoreType.DMA((second, 3))],
-            limit=4,
-        )(mixed, *experts)
+    down = call(
+        functools.partial(fetch_kernel, min(first, steps - 1) * chunk),
+        kept((chunk, width), BF16),
+        [pl.BlockSpec(memory_space=pl.ANY), hbm_spec()],
+        [pltpu.SemaphoreType.DMA],
+        limit=4,
+    )(mixed, experts[2])
 
     if 2 * share % 128:
         both = [side.transpose(1, 0, 2).reshape(half_rows, width) for side in (mixed, other_mixed)]
     else:
         both = [mixed, other_mixed]
-    left = max(steps - first - second, 1)
+    left = max(steps - first, 1)
     own, other, mine = call(
         functools.partial(expert_kernel, len(heads) // 3),
         (
@@ -620,10 +619,10 @@
             kept((chips, token_rows, width), BF16),
             kept((token_rows, width), F32),
         ),
-        [vmem_spec()] * (3 + len(heads)) + [hbm_spec()] * 3,
+        [vmem_spec()] * (4 + len(heads)) + [hbm_spec()] * 3,
         [*triple(left, pltpu.VMEM), pltpu.SemaphoreType.DMA((left, 3))],
         limit=28,
-    )(*both, ffn_row, *heads, *experts)
+    )(*both, ffn_row, down, *heads, *experts)
     other = mate(other)
     sums = call(
         combine_kernel,

time: 68.6 us -> 68.7 us (level)
  waiting for transfers between devices: 7.1 us -> 5.65 us
  Pallas kernels: 13.3 us -> 14.3 us
    ppermute x1, waiting for transfers between devices: 1.35 us -> 0.1 us  [local(): other_mixed = mate(mixed)]
    pallas_call x0 -> x1, Pallas kernels: none -> 1.23 us  [local(): call(functools.partial(fetch_kernel, min(first, steps - 1) * chunk), kept...]
  transfers between devices with their start and end apart: 7 -> 7, of which waited for: 3 -> 3; matrix products, arithmetic and copies ran while one was open for 0% -> 0% of each run, Pallas kernels for 3% -> 5%
where the time goes in v1:
time: 68.7 us; the launch traced here: 68.3 us
  blocking collectives  38.7 us (56%)
  Pallas kernels  14.3 us (21%)
  starting transfers between devices  8.88 us (13%)
  waiting for transfers between devices  5.65 us (8%)
  between operations  0.71 us (1%)
    all_to_all x1, blocking collectives, local(): sums = exchange(sums)  10.2 us
    all_to_all x1, blocking collectives, local(): mixed = exchange(mixed)  9.74 us
    all_to_all x1, blocking collectives, local(): parts = exchange(parts)  9.51 us
    all_to_all x1, blocking collectives, local(): rows = exchange(rows)  9.29 us
    all_to_all x1, starting transfers between devices, local(): exchange(tokens.reshape(token_rows, chips, 2 * share).transpose(1, 0, 2))  7.25 us
    pallas_call x1, Pallas kernels, local(): call(functools.partial(expert_kernel, len(heads) // 3), (kept((chips, tok...  6.13 us
    all_to_all x1, waiting for transfers between devices, local(): exchange(tokens.reshape(token_rows, chips, 2 * share).transpose(1, 0, 2))  4.55 us
    pallas_call x1, Pallas kernels, local(): call(attend_kernel, (kept((chips, token_rows, QUERY_WIDTH), BF16), kept((...  3.74 us
  transfers between devices with their start and end apart: 7, of which 3 were waited for; matrix products, arithmetic and copies ran while one was open for 0% of the time, Pallas kernels for 5%

profile of v1, /device:TPU:0, one launch (start us, length us, event | category | flops | bytes accessed | tf_op | source)
XLA Modules:
  0.0 68.3 jit_solution(8076299552781325665)
XLA Ops:
  0.6 0.6 collective-permute-start
  1.2 0.1 collective-permute-start.3
  1.3 0.4 collective-permute-start.1
  1.7 0.1 collective-permute-start.2
  1.8 7.2 %all-to-all-start = ((bf16[8,4,256]{2,1,0:T(4,128)(2,1)}), bf16[8,4,256]{2,1,0:T(4,128)(2,1)S(1)}, u32[]{:S(2)}, u32[]{:S(2)}) async-start(bf16[8,4,256]{2,1,0:T(4,128)(2,1)} %bitcast.9), calls=%async_computation | async-start | bytes 32768 | tf_op jit(solution)/shard_map/all_to_all | solution.py:513
  9.0 2.0 %shard_map.193 = (f32[2,128]{1,0:T(2,128)S(1)}, f32[4,128]{1,0:T(4,128)S(1)}, f32[2,128]{1,0:T(2,128)S(1)}, f32[2,256]{1,0:T(2,128)S(1)}, f32[4,128]{1,0:T(4,128...) custom-call(s32[4]{0:T(128)} %lengths_hbm.1, ...), custom_call_target="tpu_custom_call" | custom-call | tf_op jit(solution)/shard_map/pallas_call | solution.py:532
  11.1 4.5 %all-to-all-done.rows_ref.tokens_ref = bf16[8,4,256]{2,1,0:T(4,128)(2,1)S(1)} async-done(((bf16[8,4,256]{2,1,0:T(4,128)(2,1)}), bf16[8,4,256]{2,1,0:T(4,128)(2,1)S(1)}, u32[]{:S(2)}, u32[]{:S(2)}) %all-to-all-start) | async-done | bytes 16416 | tf_op jit(solution)/shard_map/all_to_all | solution.py:513
  15.6 0.0 collective-permute-done.1.wk_ref
  15.6 0.0 collective-permute-done.2.wv_ref
  15.6 0.0 collective-permute-done.wq_ref
  15.6 0.0 collective-permute-done.3.after_ref.other_ref
  15.6 0.2 shard_map.194
  15.9 9.5 %all_to_all.25.parts_ref = bf16[8,4,1536]{2,1,0:T(4,128)(2,1)S(1)} all-to-all(bf16[8,4,1536]{2,1,0:T(4,128)(2,1)S(1)} %shard_map.194), channel_id=1, replica_groups={{0,2,4,6,8,10,12,14},{1,3,5,7,9,11,13,15},{16,18,20,22,24,26,28,30},{17..., dimensions={0} | all-to-all | bytes 196608 | tf_op jit(solution)/shard_map/all_to_all | solution.py:564
  25.4 3.7 %shard_map.195 = (bf16[8,4,1024]{2,1,0:T(4,128)(2,1)S(1)}, bf16[4,256]{1,0:T(4,128)(2,1)S(1)}, bf16[4,256]{1,0:T(4,128)(2,1)S(1)}, bf16[2048,512]{1,0:T(8,128)(2...) custom-call(bf16[8,4,1536]{2,1,0:T(4,128)(2,1)S(1)} %all_to_all.25.parts_ref, ...), custom_call_target="tpu_custom_call" | custom-call | tf_op jit(solution)/shard_map/pallas_call | solution.py:576
  29.1 9.3 %all_to_all.26.rows_ref = bf16[8,4,1024]{2,1,0:T(4,128)(2,1)S(1)} all-to-all(bf16[8,4,1024]{2,1,0:T(4,128)(2,1)S(1)} %get-tuple-element.27), channel_id=1, replica_groups={{0,2,4,6,8,10,12,14},{1,3,5,7,9,11,13,15},{16,18,20,22,24,26,28,30},{17..., dimensions={0} | all-to-all | bytes 131072 | tf_op jit(solution)/shard_map/all_to_all | solution.py:592
  38.4 0.2 shard_map.196
  38.6 9.7 %all_to_all.27.after_hbm.own_mixed_ref = bf16[8,32,256]{2,1,0:T(8,128)(2,1)S(1)} all-to-all(bf16[8,32,256]{2,1,0:T(8,128)(2,1)S(1)} %shard_map.196), channel_id=1, replica_groups={{0,2,4,6,8,10,12,14},{1,3,5,7,9,11,13,15},{16,18,20,22,24,26,28,30},{17..., dimensions={0} | all-to-all | bytes 262144 | tf_op jit(solution)/shard_map/all_to_all | solution.py:600
  48.4 0.0 collective-permute-start.4
  48.4 1.2 %shard_map.197.down_ref = bf16[256,2048]{1,0:T(8,128)(2,1)S(1)} custom-call(bf16[8,32,256]{2,1,0:T(8,128)(2,1)S(1)} %all_to_all.27.after_hbm.own_mixed_ref, bf16[1792,2048]{1,0:T(8,128)(2,1)} %rest_5_.1), custom_call_target="tpu_custom_call" | custom-call | tf_op jit(solution)/shard_map/pallas_call | solution.py:602
  49.6 0.1 collective-permute-done.4.other_mixed_ref
  49.7 6.1 %shard_map.198 = (f32[8,4,2048]{2,1,0:T(4,128)S(1)}, bf16[8,4,2048]{2,1,0:T(4,128)(2,1)S(1)}, f32[4,2048]{1,0:T(4,128)S(1)}) custom-call(bf16[8,32,256]{2,1,0:T(8,128)(2,1)S(1)} %all_to_all.27.after_hbm.own_mixed_ref, bf16[8,32,256]{2,1,0:T(8,128)(2,1)S(1)} %collective-permute-done.4.other_mixed_ref, f32[1,2048]{1,0:T(1,128)S(1)} %get-tuple-element.29.gain_ref, ...), custom_call_target="tpu_custom_call" | custom-call | tf_op jit(solution)/shard_map/pallas_call | solution.py:615
  55.9 0.5 collective-permute-start.5
  56.3 1.0 %collective-permute-done.5.other_ref = bf16[8,4,2048]{2,1,0:T(4,128)(2,1)S(1)} collective-permute-done((bf16[8,4,2048]{2,1,0:T(4,128)(2,1)S(1)}, bf16[8,4,2048]{2,1,0:T(4,128)(2,1)S(1)}, u32[]{:S(2)}, u32[]{:S(2)}) %collective-permute-start.5) | collective-permute-done | bytes 131104 | tf_op jit(solution)/shard_map/ppermute | solution.py:626
  57.3 0.1 shard_map.199
  57.4 10.2 %all_to_all.28.parts_ref = bf16[8,4,2048]{2,1,0:T(4,128)(2,1)S(1)} all-to-all(bf16[8,4,2048]{2,1,0:T(4,128)(2,1)S(1)} %shard_map.199), channel_id=1, replica_groups={{0,2,4,6,8,10,12,14},{1,3,5,7,9,11,13,15},{16,18,20,22,24,26,28,30},{17..., dimensions={0} | all-to-all | bytes 262144 | tf_op jit(solution)/shard_map/all_to_all | solution.py:633
  67.6 0.7 %shard_map.200 = (bf16[4,2048]{1,0:T(4,128)(2,1)}, bf16[4,256]{1,0:T(4,128)(2,1)}, bf16[4,256]{1,0:T(4,128)(2,1)}) custom-call(bf16[8,4,2048]{2,1,0:T(4,128)(2,1)S(1)} %all_to_all.28.parts_ref, f32[4,128]{1,0:T(4,128)S(1)} %get-tuple-element.35.gate_ref, f32[4,2048]{1,0:T(4,128)S(1)} %get-tuple-element.36.mixed_ref, ...), custom_call_target="tpu_custom_call" | custom-call | tf_op jit(solution)/shard_map/pallas_call | solution.py:635
Async XLA Ops:
  0.6 15.0 %collective-permute-start = (bf16[128,1024]{1,0:T(8,128)(2,1)}, bf16[128,1024]{1,0:T(8,128)(2,1)S(1)}, u32[]{:S(2)}, u32[]{:S(2)}) collective-permute-start(bf16[128,1024]{1,0:T(8,128)(2,1)} %wq_hbm.1), channel_id=1, source_target_pairs={{0,1},{1,0},{2,3},{3,2},{4,5},{5,4},{6,7},{7,6},{8,9},{9,8},{10,11... | collective-permute-start | bytes 786440 | tf_op jit(solution)/shard_map/ppermute | solution.py:514
  1.2 14.4 %collective-permute-start.3 = (bf16[1024,128]{1,0:T(8,128)(2,1)}, bf16[1024,128]{1,0:T(8,128)(2,1)S(1)}, u32[]{:S(2)}, u32[]{:S(2)}) collective-permute-start(bf16[1024,128]{1,0:T(8,128)(2,1)} %w_out_hbm.1), channel_id=1, source_target_pairs={{0,1},{1,0},{2,3},{3,2},{4,5},{5,4},{6,7},{7,6},{8,9},{9,8},{10,11... | collective-permute-start | bytes 786440 | tf_op jit(solution)/shard_map/ppermute | solution.py:515
  1.3 14.3 %collective-permute-start.1 = (bf16[128,256]{1,0:T(8,128)(2,1)}, bf16[128,256]{1,0:T(8,128)(2,1)S(1)}, u32[]{:S(2)}, u32[]{:S(2)}) collective-permute-start(bf16[128,256]{1,0:T(8,128)(2,1)} %wk_hbm.1), channel_id=1, source_target_pairs={{0,1},{1,0},{2,3},{3,2},{4,5},{5,4},{6,7},{7,6},{8,9},{9,8},{10,11... | collective-permute-start | bytes 196616 | tf_op jit(solution)/shard_map/ppermute | solution.py:514
  1.7 13.9 %collective-permute-start.2 = (bf16[128,256]{1,0:T(8,128)(2,1)}, bf16[128,256]{1,0:T(8,128)(2,1)S(1)}, u32[]{:S(2)}, u32[]{:S(2)}) collective-permute-start(bf16[128,256]{1,0:T(8,128)(2,1)} %wv_hbm.1), channel_id=1, source_target_pairs={{0,1},{1,0},{2,3},{3,2},{4,5},{5,4},{6,7},{7,6},{8,9},{9,8},{10,11... | collective-permute-start | bytes 196616 | tf_op jit(solution)/shard_map/ppermute | solution.py:514
  1.8 13.8 %all-to-all-start = ((bf16[8,4,256]{2,1,0:T(4,128)(2,1)}), bf16[8,4,256]{2,1,0:T(4,128)(2,1)S(1)}, u32[]{:S(2)}, u32[]{:S(2)}) async-start(bf16[8,4,256]{2,1,0:T(4,128)(2,1)} %bitcast.9), calls=%async_computation | async-start | bytes 32768 | tf_op jit(solution)/shard_map/all_to_all | solution.py:513
  48.4 1.3 %collective-permute-start.4 = (bf16[8,32,256]{2,1,0:T(8,128)(2,1)S(1)}, bf16[8,32,256]{2,1,0:T(8,128)(2,1)S(1)}, u32[]{:S(2)}, u32[]{:S(2)}) collective-permute-start(bf16[8,32,256]{2,1,0:T(8,128)(2,1)S(1)} %all_to_all.27.after_hbm.own_mixed_ref), channel_id=1, source_target_pairs={{0,1},{1,0},{2,3},{3,2},{4,5},{5,4},{6,7},{7,6},{8,9},{9,8},{10,11... | collective-permute-start | bytes 393224 | tf_op jit(solution)/shard_map/ppermute | solution.py:601
  55.9 1.5 %collective-permute-start.5 = (bf16[8,4,2048]{2,1,0:T(4,128)(2,1)S(1)}, bf16[8,4,2048]{2,1,0:T(4,128)(2,1)S(1)}, u32[]{:S(2)}, u32[]{:S(2)}) collective-permute-start(bf16[8,4,2048]{2,1,0:T(4,128)(2,1)S(1)} %get-tuple-element.34), channel_id=1, source_target_pairs={{0,1},{1,0},{2,3},{3,2},{4,5},{5,4},{6,7},{7,6},{8,9},{9,8},{10,11... | collective-permute-start | bytes 393224 | tf_op jit(solution)/shard_map/ppermute | solution.py:626
